TPU v7x, 32 devices: a whole 2x2x4 slice. The times are simulated.
32 devices in a mesh: rep: 2 (over x), fs: 8 (over z, y), tp: 2 (over core).
Axes of the slice: x: 2, y: 2, z: 4, core: 2. Of those that a mesh axis runs over, the one named last changes fastest.
Arguments:
- activations: bfloat16 [16384, 1024], P(('rep', 'fs', 'tp')), may hold values from -8 to 8
- mixer_gain: float32 [1024], replicated, may hold values from 0.1 to 1.9
- query_weight: bfloat16 [1024, 256], P('fs', 'tp'), may hold values from -0.1875 to 0.1875
- key_weight: bfloat16 [1024, 256], P('fs', 'tp'), may hold values from -0.1875 to 0.1875
- value_weight: bfloat16 [1024, 512], P('fs', 'tp'), may hold values from -0.1875 to 0.1875
- rank_weight: bfloat16 [1024, 16], replicated, may hold values from -0.1875 to 0.1875
- decay_gate_weight: bfloat16 [16, 256], P(None, 'tp'), may hold values from -1.5 to 1.5
- decay_gate_bias: float32 [256], P('tp'), may hold values from -1.5 to 8
- head_gain: float32 [256], replicated, may hold values from 0.1 to 1.9
- output_weight: bfloat16 [512, 1024], P('tp', 'fs'), may hold values from -0.25 to 0.25
- ffn_gain: float32 [1024], replicated, may hold values from 0.1 to 1.9
- gate_weight: bfloat16 [1024, 2816], P('fs', 'tp'), may hold values from -0.1875 to 0.1875
- up_weight: bfloat16 [1024, 2816], P('fs', 'tp'), may hold values from -0.1875 to 0.1875
- down_weight: bfloat16 [2816, 1024], P('tp', 'fs'), may hold values from -0.109375 to 0.109375
Outputs:
- result: bfloat16 [16384, 1024], P(('rep', 'fs', 'tp'))
All inputs are finite; a program needn't handle non-finite values.
Results may differ from a plain program's by a relative error of at most 0.0056.
Values may be sent and summed in bfloat16 or wider, within the bound.
No kernel may reach another device: no remote copies, remote signals or barrier semaphores. Data moves between devices by JAX's collectives and lax.ppermute only.
A program may use at most 64 MiB of HBM per device.

v0:
```python
import jax
import jax.numpy as jnp
from jax import lax
from jax.sharding import PartitionSpec as P

DK = 128
DV = 256
BLOCK = 64
epsilon = 1e-06
decay_softness = 16.0
highest = lax.Precision.HIGHEST


def rms_scale(values, gains):
    return values * lax.rsqrt(jnp.mean(values * values, axis=-1, keepdims=True) + epsilon) * gains


def linear_attention(queries, keys_all, values_all, decay_logarithm, head_count):
    length = queries.shape[0]
    number = length // BLOCK
    halfway = BLOCK // 2
    causal = jnp.tril(jnp.ones((BLOCK, BLOCK), bool))

    def to_blocks(matrix):
        return matrix.astype(jnp.float32).reshape(
            number, BLOCK, head_count, matrix.shape[1] // head_count
        )

    block_query = to_blocks(queries)
    block_key = to_blocks(keys_all)
    block_value = to_blocks(values_all)
    cumulative = jnp.cumsum(to_blocks(decay_logarithm), axis=1)
    middle = cumulative[:, halfway - 1 : halfway]
    query_local = block_query * jnp.exp(cumulative - middle)
    key_local = block_key * jnp.exp(middle - cumulative)
    scores = jnp.einsum("nthd,nshd->nhts", query_local, key_local, precision=highest)
    scores = jnp.where(causal[None, None], scores, 0.0)
    within = jnp.einsum("nhts,nshv->nthv", scores, block_value, precision=highest)
    lasting = cumulative[:, -1]
    update = jnp.einsum(
        "nshd,nshv->nhdv",
        block_key * jnp.exp(lasting[:, None] - cumulative),
        block_value,
        precision=highest,
    )

    def advance(memory, inputs):
        fade, addition = inputs
        return (jnp.exp(fade)[:, :, None] * memory + addition, memory)

    key_width = queries.shape[1] // head_count
    value_width = values_all.shape[1] // head_count
    initial = jnp.zeros((head_count, key_width, value_width), jnp.float32)
    earlier = lax.scan(advance, initial, (lasting, update))[1]
    carried = jnp.einsum(
        "nthd,nhdv->nthv", block_query * jnp.exp(cumulative), earlier, precision=highest
    )
    return (within + carried).reshape(length, head_count, value_width)


def project_inputs(source, weight):
    return jnp.dot(source, weight, preferred_element_type=jnp.float32)


def local(
    activations,
    mixer_gain,
    query_weight,
    key_weight,
    value_weight,
    rank_weight,
    decay_gate_weight,
    decay_gate_bias,
    head_gain,
    output_weight,
    ffn_gain,
    gate_weight,
    up_weight,
    down_weight,
):
    residual = activations.astype(jnp.float32)
    normed = rms_scale(residual, mixer_gain).astype(jnp.bfloat16)
    rank_slice = project_inputs(normed, rank_weight).astype(jnp.bfloat16)
    sequence, rank_slices_gathered = (
        lax.all_gather(normed, "tp", axis=0, tiled=True),
        lax.all_gather(rank_slice, "tp", axis=0, tiled=True),
    )
    length = sequence.shape[0]
    query_full, key_full, value_full = (
        lax.all_gather(query_weight, "fs", axis=0, tiled=True),
        lax.all_gather(key_weight, "fs", axis=0, tiled=True),
        lax.all_gather(value_weight, "fs", axis=0, tiled=True),
    )
    queries = project_inputs(sequence, query_full).astype(jnp.bfloat16)
    keys_all = project_inputs(sequence, key_full).astype(jnp.bfloat16)
    values_all = project_inputs(sequence, value_full).astype(jnp.bfloat16)
    decay_logarithm = (
        jax.nn.log_sigmoid(
            project_inputs(rank_slices_gathered, decay_gate_weight) + decay_gate_bias
        )
        / decay_softness
    )
    head_count = query_weight.shape[1] // DK
    attended = linear_attention(queries, keys_all, values_all, decay_logarithm, head_count)
    head_rows = rms_scale(attended, head_gain).astype(jnp.bfloat16).reshape(length, head_count * DV)
    own_rows = lax.all_to_all(head_rows, "tp", split_axis=0, concat_axis=1, tiled=True)
    tall_out = lax.all_gather(output_weight, "tp", axis=0, tiled=True)
    whole_out = lax.all_gather(tall_out, "fs", axis=1, tiled=True)
    mixed = residual + project_inputs(own_rows, whole_out)
    ffn_normed = rms_scale(mixed, ffn_gain).astype(jnp.bfloat16)
    ffn_sequence = lax.all_gather(ffn_normed, "tp", axis=0, tiled=True)
    gate_full, up_full = (
        lax.all_gather(gate_weight, "fs", axis=0, tiled=True),
        lax.all_gather(up_weight, "fs", axis=0, tiled=True),
    )
    down_full = lax.all_gather(down_weight, "fs", axis=1, tiled=True)
    hidden = (
        jax.nn.silu(project_inputs(ffn_sequence, gate_full)) * project_inputs(ffn_sequence, up_full)
    ).astype(jnp.bfloat16)
    result = mixed + lax.psum_scatter(
        project_inputs(hidden, down_full).astype(jnp.bfloat16),
        "tp",
        scatter_dimension=0,
        tiled=True,
    ).astype(jnp.float32)
    return result.astype(jnp.bfloat16)


def solution(mesh):
    in_specs = (
        P(("rep", "fs", "tp"), None),
        P(),
        P("fs", "tp"),
        P("fs", "tp"),
        P("fs", "tp"),
        P(),
        P(None, "tp"),
        P("tp"),
        P(),
        P("tp", "fs"),
        P(),
        P("fs", "tp"),
        P("fs", "tp"),
        P("tp", "fs"),
    )
    out_specs = P(("rep", "fs", "tp"), None)
    return jax.shard_map(local, mesh=mesh, in_specs=in_specs, out_specs=out_specs, check_vma=False)
```

profile of v0, /device:TPU:0, one launch (start us, length us, event | category | flops | bytes accessed | tf_op | source)
XLA Modules:
  0.0 369.9 jit_solution(17549334003282702146)
XLA Ops:
  6.5 1.5 fusion.2
  8.1 2.5 fusion.4
  10.7 2.2 all_gather.38
  13.0 1.6 convolution_convert_fusion.3
  14.6 2.1 all_gather.36
  16.8 0.5 fusion.12
  17.2 0.3 fusion.24
  17.6 32.6 %all_gather.37 = bf16[1024,128]{1,0:T(8,128)(2,1)S(1)} all-gather(bf16[128,128]{1,0:T(8,128)(2,1)S(1)} %copy-done.8), channel_id=1, replica_groups=mesh['rep'=2,'fs'=8,'tp'=2] {'fs'}, dimensions={0}, use_global_device_ids=true | all-gather | bytes 294912 | tf_op jit(solution)/shard_map/all_gather | solution.py:91
  50.2 31.1 %all_gather.35 = bf16[1024,128]{1,0:T(8,128)(2,1)S(1)} all-gather(bf16[128,128]{1,0:T(8,128)(2,1)S(1)} %copy-done.9), channel_id=1, replica_groups=mesh['rep'=2,'fs'=8,'tp'=2] {'fs'}, dimensions={0}, use_global_device_ids=true | all-gather | bytes 294912 | tf_op jit(solution)/shard_map/all_gather | solution.py:90
  81.3 31.3 %all_gather.34 = bf16[1024,256]{1,0:T(8,128)(2,1)S(1)} all-gather(bf16[128,256]{1,0:T(8,128)(2,1)S(1)} %copy-done.7), channel_id=1, replica_groups=mesh['rep'=2,'fs'=8,'tp'=2] {'fs'}, dimensions={0}, use_global_device_ids=true | all-gather | bytes 589824 | tf_op jit(solution)/shard_map/all_gather | solution.py:92
  112.6 2.4 convolution_convert_fusion.1
  115.1 0.7 convolution_convert_fusion.2
  115.8 1.6 fusion.14
  117.4 0.7 convolution_convert_fusion
  118.1 1.1 convolution_bitcast_fusion
  119.2 12.6 %while.13 = (s32[]{:T(128)}, f32[1,128,256]{2,1,0:T(8,128)S(1)}, f32[16,1,128,256]{3,2,1,0:T(8,128)}, f32[16,1,128]{2,1,0:T(1,128)S(1)}, f32[16,1,128,256]{3,2,1,0:T(8,128)S(1)}, /*index=5*/s32[]{:T(128)}, s32[]{:T(128)}) while((s32[]{:T(128)}, f32[1,128,256]{2,1,0:T(8,128)S(1)}, f32[16,1,128,256]{3,2,1,0:T(8,128)}, ...), condition=%wide.region_3.4_spmd.clone, body=%wide.region_2.3_spmd.clone.sunk | while | flops 131075 | bytes 657504 | solution.py:54
  119.2 0.7 bitcast_dynamic-update-slice_fusion.2
  119.9 0.1 bitcast_add_fusion.2
  120.0 0.7 bitcast_dynamic-update-slice_fusion.2
  120.7 0.1 bitcast_add_fusion.2
  120.8 0.7 bitcast_dynamic-update-slice_fusion.2
  121.4 0.1 bitcast_add_fusion.2
  121.6 0.7 bitcast_dynamic-update-slice_fusion.2
  122.2 0.1 bitcast_add_fusion.2
  122.3 0.7 bitcast_dynamic-update-slice_fusion.2
  123.0 0.1 bitcast_add_fusion.2
  123.1 0.7 bitcast_dynamic-update-slice_fusion.2
  123.8 0.1 bitcast_add_fusion.2
  123.9 0.6 bitcast_dynamic-update-slice_fusion.2
  124.6 0.1 bitcast_add_fusion.2
  124.7 0.7 bitcast_dynamic-update-slice_fusion.2
  125.4 0.1 bitcast_add_fusion.2
  125.5 0.7 bitcast_dynamic-update-slice_fusion.2
  126.2 0.1 bitcast_add_fusion.2
  126.3 0.7 bitcast_dynamic-update-slice_fusion.2
  127.1 0.7 bitcast_dynamic-update-slice_fusion.2
  127.7 0.1 bitcast_add_fusion.2
  127.9 0.7 bitcast_dynamic-update-slice_fusion.2
  128.7 0.7 bitcast_dynamic-update-slice_fusion.2
  129.4 0.7 bitcast_dynamic-update-slice_fusion.2
  130.2 0.7 bitcast_dynamic-update-slice_fusion.2
  131.0 0.7 bitcast_dynamic-update-slice_fusion.2
  131.8 2.2 convolution_select_fusion
  134.1 3.0 fusion.5
  137.1 0.7 fusion.10
  137.8 0.3 copy.33
  138.3 0.9 multiply_convert_fusion.2
  139.2 3.5 all-to-all-start
  142.8 1.7 all-to-all-done
  144.4 0.8 copy-done.3
  145.2 2.2 multiply_reduce_fusion
  147.5 1.2 multiply_convert_fusion.1
  148.7 0.5 all-gather.13.cloned.1.call-update
  149.3 0.5 all-gather.15.cloned.1.call-update
  149.9 0.5 all-gather.17.cloned.1.call-update
  150.4 0.2 reduce-scatter.2.cloned.1.call-start
  150.7 10.0 %all-gather.11.cloned.1.call-done = bf16[1024,1024]{1,0:T(8,128)(2,1)} async-done(((bf16[512,1024]{1,0:T(8,128)(2,1)}), bf16[1024,1024]{1,0:T(8,128)(2,1)}) %all-gather.11.cloned.1.call-update) | async-done | bytes 2097168 | tf_op jit(solution)/shard_map/all_gather | solution.py:111
  160.7 60.5 %all-gather.13.cloned.1.call-done = bf16[1024,1408]{1,0:T(8,128)(2,1)} async-done(((bf16[128,1408]{1,0:T(8,128)(2,1)}), bf16[1024,1408]{1,0:T(8,128)(2,1)}) %all-gather.13.cloned.1.call-update) | async-done | bytes 2883600 | tf_op jit(solution)/shard_map/all_gather | solution.py:113
  221.2 8.3 %fusion.27 = f32[1024,1408]{1,0:T(8,128)} fusion(bf16[1024,1024]{1,0:T(8,128)(2,1)} %all-gather.11.cloned.1.call-done, bf16[1024,1408]{1,0:T(8,128)(2,1)} %all-gather.13.cloned.1.call-done), kind=kOutput, calls=%fused_computation.58 | convolution fusion | flops 2952790016 | bytes 10747904 | tf_op jit(solution)/shard_map/dot_general | solution.py:62
  229.6 49.6 %all-gather.15.cloned.1.call-done = bf16[1024,1408]{1,0:T(8,128)(2,1)} async-done(((bf16[128,1408]{1,0:T(8,128)(2,1)}), bf16[1024,1408]{1,0:T(8,128)(2,1)}) %all-gather.15.cloned.1.call-update) | async-done | bytes 2883600 | tf_op jit(solution)/shard_map/all_gather | solution.py:114
  279.2 60.1 %all-gather.17.cloned.1.call-done = bf16[1408,1024]{1,0:T(8,128)(2,1)} async-done(((bf16[1408,128]{1,0:T(8,128)(2,1)}), bf16[1408,1024]{1,0:T(8,128)(2,1)}) %all-gather.17.cloned.1.call-update) | async-done | bytes 2883600 | tf_op jit(solution)/shard_map/all_gather | solution.py:116
  339.3 13.1 %fusion.8 = bf16[1024,1024]{1,0:T(8,128)(2,1)} fusion(bf16[1408,1024]{1,0:T(8,128)(2,1)} %all-gather.17.cloned.1.call-done, f32[1024,1408]{1,0:T(8,128)} %fusion.27, bf16[1024,1024]{1,0:T(8,128)(2,1)} %all-gather.11.cloned.1.call-done, bf16[1024,1408]{1,0:T(8,128)(2,1)} %all-gather.15.cloned.1.call-done), kind=kOutput, calls=%fused_computation.18 | convolution fusion | flops 5915279360 | bytes 15728640 | tf_op jit(solution)/shard_map/dot_general | solution.py:62
  352.4 8.1 %reduce-scatter.2.cloned.1.call-done = bf16[512,1024]{1,0:T(8,128)(2,1)} async-done(((bf16[1024,1024]{1,0:T(8,128)(2,1)}), bf16[512,1024]{1,0:T(8,128)(2,1)}) %reduce-scatter.2.cloned.1.call-update) | async-done | bytes 1048592 | tf_op jit(solution)/shard_map/reduce_scatter | solution.py:120
  360.5 2.5 add_convert_fusion
  (71 shorter events, 1.2 us)
Async XLA Ops:
  6.5 6.4 %copy-start = (bf16[1024,16]{0,1:T(8,128)(2,1)S(1)}, bf16[1024,16]{0,1:T(8,128)(2,1)}, u32[]{:S(2)}) copy-start(bf16[1024,16]{0,1:T(8,128)(2,1)} %param.21) | copy-start | bytes 98308
  6.5 106.0 %all-gather.7.cloned.1.call-start = ((), (), s32[]{:S(2)}) async-start(), calls=%async_computation.2 | async-start | bytes 3145728 | tf_op jit(solution)/shard_map/all_gather | solution.py:85
  6.5 4.2 %copy-start.6 = (bf16[256,128]{1,0:T(8,128)(2,1)S(1)}, bf16[256,128]{1,0:T(8,128)(2,1)}, u32[]{:S(2)}) copy-start(bf16[256,128]{1,0:T(8,128)(2,1)} %param.25) | copy-start | bytes 196612
  8.1 8.7 %copy-start.12 = (bf16[16,128]{1,0:T(8,128)(2,1)S(1)}, bf16[16,128]{1,0:T(8,128)(2,1)}, u32[]{:S(2)}) copy-start(bf16[16,128]{1,0:T(8,128)(2,1)} %param.22) | copy-start | bytes 12292
  8.1 8.7 %copy-start.13 = (f32[128]{0:T(128)S(1)}, f32[128]{0:T(128)}, u32[]{:S(2)}) copy-start(f32[128]{0:T(128)} %param.23) | copy-start | bytes 1540
  10.7 132.1 %all-gather.9.cloned.1.call-start = ((), (), s32[]{:S(2)}) async-start(), calls=%async_computation.3 | async-start | bytes 1179648 | tf_op jit(solution)/shard_map/all_gather | solution.py:108
  13.0 4.6 %copy-start.8 = (bf16[128,128]{1,0:T(8,128)(2,1)S(1)}, bf16[128,128]{1,0:T(8,128)(2,1)}, u32[]{:S(2)}) copy-start(bf16[128,128]{1,0:T(8,128)(2,1)} %param.19) | copy-start | bytes 98308
  14.6 35.6 %copy-start.9 = (bf16[128,128]{1,0:T(8,128)(2,1)S(1)}, bf16[128,128]{1,0:T(8,128)(2,1)}, u32[]{:S(2)}) copy-start(bf16[128,128]{1,0:T(8,128)(2,1)} %param.18) | copy-start | bytes 98308
  14.6 66.6 %copy-start.7 = (bf16[128,256]{1,0:T(8,128)(2,1)S(1)}, bf16[128,256]{1,0:T(8,128)(2,1)}, u32[]{:S(2)}) copy-start(bf16[128,256]{1,0:T(8,128)(2,1)} %param.20) | copy-start | bytes 196612
  112.6 2.5 copy-start.2
  118.1 1.1 copy-start.4
  134.0 3.0 copy-start.5
  137.1 1.2 copy-start.11
  137.8 7.4 %copy-start.1 = (bf16[512,1024]{1,0:T(8,128)(2,1)S(1)}, bf16[512,1024]{1,0:T(8,128)(2,1)}, u32[]{:S(2)}) copy-start(bf16[512,1024]{1,0:T(8,128)(2,1)} %param.16) | copy-start | bytes 3145732
  139.2 5.2 %all-to-all-start = ((bf16[2,512,256]{1,2,0:T(8,128)(2,1)}), bf16[2,512,256]{1,2,0:T(8,128)(2,1)S(1)}, u32[]{:S(2)}, u32[]{:S(2)}) async-start(bf16[2,512,256]{1,2,0:T(8,128)(2,1)} %multiply_convert_fusion.2), calls=%async_computation | async-start | bytes 1048576 | tf_op jit(solution)/shard_map/all_to_all | solution.py:106
  142.7 18.0 %all-gather.11.cloned.1.call-start = ((), (), s32[]{:S(2)}) async-start(), calls=%async_computation.4 | async-start | bytes 3145728 | tf_op jit(solution)/shard_map/all_gather | solution.py:111
  144.4 0.8 copy-start.3
  145.2 2.2 copy-start.10
  148.7 72.5 %all-gather.13.cloned.1.call-start = ((), (), s32[]{:S(2)}) async-start(), calls=%async_computation.5 | async-start | bytes 3244032 | tf_op jit(solution)/shard_map/all_gather | solution.py:113
  149.3 129.9 %all-gather.15.cloned.1.call-start = ((), (), s32[]{:S(2)}) async-start(), calls=%async_computation.6 | async-start | bytes 3244032 | tf_op jit(solution)/shard_map/all_gather | solution.py:114
  149.9 189.5 %all-gather.17.cloned.1.call-start = ((), (), s32[]{:S(2)}) async-start(), calls=%async_computation.7 | async-start | bytes 3244032 | tf_op jit(solution)/shard_map/all_gather | solution.py:116
  150.4 210.1 %reduce-scatter.2.cloned.1.call-start = ((), (), s32[]{:S(2)}) async-start(), calls=%async_computation.8 | async-start | bytes 3145728 | tf_op jit(solution)/shard_map/reduce_scatter | solution.py:120
Sparse Core Ops, SparseCore 0:
  10.8 13.2 all-gather.6
  26.1 42.2 all-gather.8
  148.8 11.8 all-gather.10
  162.7 58.4 all-gather.12
  223.3 55.9 all-gather.14
  281.1 58.1 all-gather.16
  352.5 7.9 reduce-scatter.1
where the time goes:
time: 370 us
  waiting for transfers between devices  192 us (52%)
  blocking collectives  99.3 us (27%)
  matrix products  36.6 us (10%)
  other arithmetic  22.9 us (6%)
  between operations  13.8 us (4%)
  starting transfers between devices  3.91 us (1%)
    all_gather x1, waiting for transfers between devices, local(): lax.all_gather(gate_weight, 'fs', axis=0, tiled=True)  60.5 us
    all_gather x1, waiting for transfers between devices, local(): down_full = lax.all_gather(down_weight, 'fs', axis=1, tiled=True)  60.1 us
    all_gather x1, waiting for transfers between devices, local(): lax.all_gather(up_weight, 'fs', axis=0, tiled=True)  49.6 us
    all_gather x1, blocking collectives, local(): lax.all_gather(key_weight, 'fs', axis=0, tiled=True)  32.6 us
    all_gather x1, blocking collectives, local(): lax.all_gather(value_weight, 'fs', axis=0, tiled=True)  31.3 us
    all_gather x1, blocking collectives, local(): lax.all_gather(query_weight, 'fs', axis=0, tiled=True)  31.1 us
    dot_general x8, matrix products, project_inputs(): return jnp.dot(source, weight, preferred_element_type=jnp.float32)  29.6 us
    dynamic_update_slice x16, other arithmetic, linear_attention(): earlier = lax.scan(advance, initial, (lasting, update))[1]  10.6 us
  transfers between devices with their start and end apart: 8, of which 6 were waited for; matrix products, arithmetic and copies ran while one was open for 10% of the time, Pallas kernels for 0%

commit v1 on v0

--- a/solution.py
+++ b/solution.py
@@ -87,7 +87,9 @@
     )
     length = sequence.shape[0]
     query_full, key_full, value_full = (
-        lax.all_gather(query_weight, "fs", axis=0, tiled=True),
+        jnp.concatenate(
+            lax.all_to_all(jnp.stack([query_weight] * lax.axis_size("fs")), "fs", 0, 0), axis=0
+        ),
         lax.all_gather(key_weight, "fs", axis=0, tiled=True),
         lax.all_gather(value_weight, "fs", axis=0, tiled=True),
     )

time: 370 us -> 346 us (0.935)
  blocking collectives: 99.3 us -> 67.8 us
  starting transfers between devices: 3.91 us -> 11.2 us
    all_gather x1 -> x0, blocking collectives: 31.1 us -> none  [local(): lax.all_gather(query_weight, 'fs', axis=0, tiled=True)]
    all_to_all x0 -> x1, starting transfers between devices: none -> 7.31 us  [local(): lax.all_to_all(jnp.stack([query_weight] * lax.axis_size('fs')), 'fs', 0, 0)]
  transfers between devices with their start and end apart: 8 -> 9, of which waited for: 6 -> 6; matrix products, arithmetic and copies ran while one was open for 10% -> 11% of each run, Pallas kernels for 0% -> 0%
where the time goes in v1:
time: 346 us; the launch traced here: 345 us
  waiting for transfers between devices  192 us (55%)
  blocking collectives  67.8 us (20%)
  matrix products  35.4 us (10%)
  other arithmetic  23 us (7%)
  between operations  13.8 us (4%)
  starting transfers between devices  11.2 us (3%)
    all_gather x1, waiting for transfers between devices, local(): lax.all_gather(gate_weight, 'fs', axis=0, tiled=True)  60.5 us
    all_gather x1, waiting for transfers between devices, local(): down_full = lax.all_gather(down_weight, 'fs', axis=1, tiled=True)  60.1 us
    all_gather x1, waiting for transfers between devices, local(): lax.all_gather(up_weight, 'fs', axis=0, tiled=True)  49.6 us
    all_gather x1, blocking collectives, local(): lax.all_gather(value_weight, 'fs', axis=0, tiled=True)  31.9 us
    all_gather x1, blocking collectives, local(): lax.all_gather(key_weight, 'fs', axis=0, tiled=True)  31.5 us
    dot_general x8, matrix products, project_inputs(): return jnp.dot(source, weight, preferred_element_type=jnp.float32)  28.3 us
    dynamic_update_slice x16, other arithmetic, linear_attention(): earlier = lax.scan(advance, initial, (lasting, update))[1]  10.6 us
    all_gather x1, waiting for transfers between devices, local(): ffn_sequence = lax.all_gather(ffn_normed, 'tp', axis=0, tiled=True)  9.87 us
  transfers between devices with their start and end apart: 9, of which 6 were waited for; matrix products, arithmetic and copies ran while one was open for 11% of the time, Pallas kernels for 0%

profile of v1, /device:TPU:0, one launch (start us, length us, event | category | flops | bytes accessed | tf_op | source)
XLA Modules:
  0.0 345.2 jit_solution(13370195524275406262)
XLA Ops:
  6.5 1.5 fusion.2
  8.1 2.5 fusion.4
  10.7 0.7 stack.2
  11.4 7.3 %all-to-all-start = ((bf16[8,128,128]{2,1,0:T(8,128)(2,1)}), bf16[8,128,128]{2,1,0:T(8,128)(2,1)S(1)}, u32[]{:S(2)}, u32[]{:S(2)}) async-start(bf16[8,128,128]{2,1,0:T(8,128)(2,1)} %stack.2), calls=%async_computation | async-start | bytes 524288 | tf_op jit(solution)/shard_map/all_to_all | solution.py:91
  18.8 2.0 all_gather.34
  20.9 0.4 convolution_convert_fusion.3
  21.3 2.3 all_gather.32
  23.6 0.5 fusion.12
  24.1 0.3 fusion.24
  24.4 31.5 %all_gather.33 = bf16[1024,128]{1,0:T(8,128)(2,1)S(1)} all-gather(bf16[128,128]{1,0:T(8,128)(2,1)S(1)} %copy-done.10), channel_id=1, replica_groups=mesh['rep'=2,'fs'=8,'tp'=2] {'fs'}, dimensions={0}, use_global_device_ids=true | all-gather | bytes 294912 | tf_op jit(solution)/shard_map/all_gather | solution.py:93
  56.0 31.9 %all_gather.31 = bf16[1024,256]{1,0:T(8,128)(2,1)S(1)} all-gather(bf16[128,256]{1,0:T(8,128)(2,1)S(1)} %copy-done.8), channel_id=1, replica_groups=mesh['rep'=2,'fs'=8,'tp'=2] {'fs'}, dimensions={0}, use_global_device_ids=true | all-gather | bytes 589824 | tf_op jit(solution)/shard_map/all_gather | solution.py:94
  87.9 2.4 convolution_convert_fusion.2
  90.4 0.7 convolution_convert_fusion.1
  91.1 1.6 fusion.14
  92.7 0.7 convolution_convert_fusion
  93.4 1.1 convolution_bitcast_fusion
  94.5 12.7 %while.13 = (s32[]{:T(128)}, f32[1,128,256]{2,1,0:T(8,128)S(1)}, f32[16,1,128,256]{3,2,1,0:T(8,128)}, f32[16,1,128]{2,1,0:T(1,128)S(1)}, f32[16,1,128,256]{3,2,1,0:T(8,128)S(1)}, /*index=5*/s32[]{:T(128)}, s32[]{:T(128)}) while((s32[]{:T(128)}, f32[1,128,256]{2,1,0:T(8,128)S(1)}, f32[16,1,128,256]{3,2,1,0:T(8,128)}, ...), condition=%wide.region_3.4_spmd.clone, body=%wide.region_2.3_spmd.clone.sunk | while | flops 131075 | bytes 657504 | solution.py:54
  94.5 0.7 bitcast_dynamic-update-slice_fusion.2
  95.3 0.7 bitcast_dynamic-update-slice_fusion.2
  96.0 0.1 bitcast_add_fusion.2
  96.1 0.7 bitcast_dynamic-update-slice_fusion.2
  96.8 0.1 bitcast_add_fusion.2
  96.9 0.7 bitcast_dynamic-update-slice_fusion.2
  97.6 0.1 bitcast_add_fusion.2
  97.7 0.7 bitcast_dynamic-update-slice_fusion.2
  98.4 0.1 bitcast_add_fusion.2
  98.5 0.7 bitcast_dynamic-update-slice_fusion.2
  99.2 0.1 bitcast_add_fusion.2
  99.3 0.7 bitcast_dynamic-update-slice_fusion.2
  100.0 0.1 bitcast_add_fusion.2
  100.1 0.7 bitcast_dynamic-update-slice_fusion.2
  100.9 0.7 bitcast_dynamic-update-slice_fusion.2
  101.5 0.1 bitcast_add_fusion.2
  101.7 0.7 bitcast_dynamic-update-slice_fusion.2
  102.4 0.7 bitcast_dynamic-update-slice_fusion.2
  103.1 0.1 bitcast_add_fusion.2
  103.2 0.7 bitcast_dynamic-update-slice_fusion.2
  103.9 0.1 bitcast_add_fusion.2
  104.0 0.7 bitcast_dynamic-update-slice_fusion.2
  104.8 0.7 bitcast_dynamic-update-slice_fusion.2
  105.6 0.7 bitcast_dynamic-update-slice_fusion.2
  106.4 0.7 bitcast_dynamic-update-slice_fusion.2
  107.2 2.2 convolution_select_fusion
  109.5 3.0 fusion.5
  112.5 0.7 fusion.10
  113.2 0.3 copy.33
  113.7 0.9 multiply_convert_fusion.2
  114.6 3.5 %all-to-all-start.1 = ((bf16[2,512,256]{1,2,0:T(8,128)(2,1)}), bf16[2,512,256]{1,2,0:T(8,128)(2,1)S(1)}, u32[]{:S(2)}, u32[]{:S(2)}) async-start(bf16[2,512,256]{1,2,0:T(8,128)(2,1)} %multiply_convert_fusion.2), calls=%async_computation.1 | async-start | bytes 1048576 | tf_op jit(solution)/shard_map/all_to_all | solution.py:108
  118.2 1.7 all-to-all-done.1
  119.8 0.8 copy-done.4
  120.6 2.2 multiply_reduce_fusion
  122.9 1.2 multiply_convert_fusion.1
  124.2 0.5 all-gather.13.cloned.1.call-update
  124.7 0.5 all-gather.15.cloned.1.call-update
  125.3 0.5 all-gather.17.cloned.1.call-update
  125.8 0.2 reduce-scatter.2.cloned.1.call-start
  126.1 9.9 %all-gather.11.cloned.1.call-done = bf16[1024,1024]{1,0:T(8,128)(2,1)} async-done(((bf16[512,1024]{1,0:T(8,128)(2,1)}), bf16[1024,1024]{1,0:T(8,128)(2,1)}) %all-gather.11.cloned.1.call-update) | async-done | bytes 2097168 | tf_op jit(solution)/shard_map/all_gather | solution.py:113
  135.9 60.5 %all-gather.13.cloned.1.call-done = bf16[1024,1408]{1,0:T(8,128)(2,1)} async-done(((bf16[128,1408]{1,0:T(8,128)(2,1)}), bf16[1024,1408]{1,0:T(8,128)(2,1)}) %all-gather.13.cloned.1.call-update) | async-done | bytes 2883600 | tf_op jit(solution)/shard_map/all_gather | solution.py:115
  196.5 8.3 %fusion.27 = f32[1024,1408]{1,0:T(8,128)} fusion(bf16[1024,1024]{1,0:T(8,128)(2,1)} %all-gather.11.cloned.1.call-done, bf16[1024,1408]{1,0:T(8,128)(2,1)} %all-gather.13.cloned.1.call-done), kind=kOutput, calls=%fused_computation.58 | convolution fusion | flops 2952790016 | bytes 10747904 | tf_op jit(solution)/shard_map/dot_general | solution.py:62
  204.8 49.6 %all-gather.15.cloned.1.call-done = bf16[1024,1408]{1,0:T(8,128)(2,1)} async-done(((bf16[128,1408]{1,0:T(8,128)(2,1)}), bf16[1024,1408]{1,0:T(8,128)(2,1)}) %all-gather.15.cloned.1.call-update) | async-done | bytes 2883600 | tf_op jit(solution)/shard_map/all_gather | solution.py:116
  254.5 60.1 %all-gather.17.cloned.1.call-done = bf16[1408,1024]{1,0:T(8,128)(2,1)} async-done(((bf16[1408,128]{1,0:T(8,128)(2,1)}), bf16[1408,1024]{1,0:T(8,128)(2,1)}) %all-gather.17.cloned.1.call-update) | async-done | bytes 2883600 | tf_op jit(solution)/shard_map/all_gather | solution.py:118
  314.6 13.0 %fusion.8 = bf16[1024,1024]{1,0:T(8,128)(2,1)} fusion(bf16[1408,1024]{1,0:T(8,128)(2,1)} %all-gather.17.cloned.1.call-done, f32[1024,1408]{1,0:T(8,128)} %fusion.27, bf16[1024,1024]{1,0:T(8,128)(2,1)} %all-gather.11.cloned.1.call-done, bf16[1024,1408]{1,0:T(8,128)(2,1)} %all-gather.15.cloned.1.call-done), kind=kOutput, calls=%fused_computation.18 | convolution fusion | flops 5915279360 | bytes 15728640 | tf_op jit(solution)/shard_map/dot_general | solution.py:62
  327.7 8.1 %reduce-scatter.2.cloned.1.call-done = bf16[512,1024]{1,0:T(8,128)(2,1)} async-done(((bf16[1024,1024]{1,0:T(8,128)(2,1)}), bf16[512,1024]{1,0:T(8,128)(2,1)}) %reduce-scatter.2.cloned.1.call-update) | async-done | bytes 1048592 | tf_op jit(solution)/shard_map/reduce_scatter | solution.py:122
  335.8 2.5 add_convert_fusion
  (75 shorter events, 1.3 us)
Async XLA Ops:
  6.5 14.3 %copy-start = (bf16[1024,16]{0,1:T(8,128)(2,1)S(1)}, bf16[1024,16]{0,1:T(8,128)(2,1)}, u32[]{:S(2)}) copy-start(bf16[1024,16]{0,1:T(8,128)(2,1)} %param.21) | copy-start | bytes 98308
  6.5 81.3 %all-gather.7.cloned.1.call-start = ((), (), s32[]{:S(2)}) async-start(), calls=%async_computation.3 | async-start | bytes 3145728 | tf_op jit(solution)/shard_map/all_gather | solution.py:85
  6.5 4.1 %copy-start.9 = (bf16[128,128]{1,0:T(8,128)(2,1)S(1)}, bf16[128,128]{1,0:T(8,128)(2,1)}, u32[]{:S(2)}) copy-start(bf16[128,128]{1,0:T(8,128)(2,1)} %param.18) | copy-start | bytes 98308
  8.1 10.7 %copy-start.7 = (bf16[256,128]{1,0:T(8,128)(2,1)S(1)}, bf16[256,128]{1,0:T(8,128)(2,1)}, u32[]{:S(2)}) copy-start(bf16[256,128]{1,0:T(8,128)(2,1)} %param.25) | copy-start | bytes 196612
  10.6 10.2 %copy-start.3 = (bf16[512,1024]{1,0:T(8,128)(2,1)S(1)}, bf16[512,1024]{1,0:T(8,128)(2,1)}, u32[]{:S(2)}) copy-start(bf16[512,1024]{1,0:T(8,128)(2,1)} %fusion.4) | copy-start | bytes 3145732
  10.6 13.0 %copy-start.13 = (bf16[16,128]{1,0:T(8,128)(2,1)S(1)}, bf16[16,128]{1,0:T(8,128)(2,1)}, u32[]{:S(2)}) copy-start(bf16[16,128]{1,0:T(8,128)(2,1)} %param.22) | copy-start | bytes 12292
  10.6 13.0 %copy-start.14 = (f32[128]{0:T(128)S(1)}, f32[128]{0:T(128)}, u32[]{:S(2)}) copy-start(f32[128]{0:T(128)} %param.23) | copy-start | bytes 1540
  11.4 76.5 %all-to-all-start = ((bf16[8,128,128]{2,1,0:T(8,128)(2,1)}), bf16[8,128,128]{2,1,0:T(8,128)(2,1)S(1)}, u32[]{:S(2)}, u32[]{:S(2)}) async-start(bf16[8,128,128]{2,1,0:T(8,128)(2,1)} %stack.2), calls=%async_computation | async-start | bytes 524288 | tf_op jit(solution)/shard_map/all_to_all | solution.py:91
  18.7 99.5 %all-gather.9.cloned.1.call-start = ((), (), s32[]{:S(2)}) async-start(), calls=%async_computation.4 | async-start | bytes 1179648 | tf_op jit(solution)/shard_map/all_gather | solution.py:110
  20.9 3.5 %copy-start.10 = (bf16[128,128]{1,0:T(8,128)(2,1)S(1)}, bf16[128,128]{1,0:T(8,128)(2,1)}, u32[]{:S(2)}) copy-start(bf16[128,128]{1,0:T(8,128)(2,1)} %param.19) | copy-start | bytes 98308
  21.3 34.7 %copy-start.8 = (bf16[128,256]{1,0:T(8,128)(2,1)S(1)}, bf16[128,256]{1,0:T(8,128)(2,1)}, u32[]{:S(2)}) copy-start(bf16[128,256]{1,0:T(8,128)(2,1)} %param.20) | copy-start | bytes 196612
  87.9 2.5 copy-start.2
  93.4 1.1 copy-start.5
  109.5 3.0 copy-start.6
  112.5 1.2 copy-start.12
  113.2 7.4 %copy-start.1 = (bf16[512,1024]{1,0:T(8,128)(2,1)S(1)}, bf16[512,1024]{1,0:T(8,128)(2,1)}, u32[]{:S(2)}) copy-start(bf16[512,1024]{1,0:T(8,128)(2,1)} %param.16) | copy-start | bytes 3145732
  114.6 5.2 %all-to-all-start.1 = ((bf16[2,512,256]{1,2,0:T(8,128)(2,1)}), bf16[2,512,256]{1,2,0:T(8,128)(2,1)S(1)}, u32[]{:S(2)}, u32[]{:S(2)}) async-start(bf16[2,512,256]{1,2,0:T(8,128)(2,1)} %multiply_convert_fusion.2), calls=%async_computation.1 | async-start | bytes 1048576 | tf_op jit(solution)/shard_map/all_to_all | solution.py:108
  118.1 17.8 %all-gather.11.cloned.1.call-start = ((), (), s32[]{:S(2)}) async-start(), calls=%async_computation.5 | async-start | bytes 3145728 | tf_op jit(solution)/shard_map/all_gather | solution.py:113
  119.8 0.8 copy-start.4
  120.6 2.2 copy-start.11
  124.1 72.4 %all-gather.13.cloned.1.call-start = ((), (), s32[]{:S(2)}) async-start(), calls=%async_computation.6 | async-start | bytes 3244032 | tf_op jit(solution)/shard_map/all_gather | solution.py:115
  124.7 129.8 %all-gather.15.cloned.1.call-start = ((), (), s32[]{:S(2)}) async-start(), calls=%async_computation.7 | async-start | bytes 3244032 | tf_op jit(solution)/shard_map/all_gather | solution.py:116
  125.3 189.3 %all-gather.17.cloned.1.call-start = ((), (), s32[]{:S(2)}) async-start(), calls=%async_computation.8 | async-start | bytes 3244032 | tf_op jit(solution)/shard_map/all_gather | solution.py:118
  125.8 209.9 %reduce-scatter.2.cloned.1.call-start = ((), (), s32[]{:S(2)}) async-start(), calls=%async_computation.9 | async-start | bytes 3145728 | tf_op jit(solution)/shard_map/reduce_scatter | solution.py:122
Sparse Core Ops, SparseCore 0:
  10.8 13.4 all-gather.6
  26.3 43.2 all-gather.8
  124.2 11.6 all-gather.10
  138.0 58.4 all-gather.12
  198.5 55.9 all-gather.14
  256.4 58.1 all-gather.16
  327.8 7.9 reduce-scatter.1
